TPU v7x, 32 devices: a whole 2x2x4 slice. The times are simulated.
32 devices in a mesh: fs: 8 (over z, y), tp: 4 (over x, core).
Axes of the slice: x: 2, y: 2, z: 4, core: 2. Of those that a mesh axis runs over, the one named last changes fastest.
Arguments:
- tokens: bfloat16 [8192, 2048], P('fs'), may hold values from -6 to 6
- norm_gain: float32 [2048], replicated, may hold values from 0.1 to 1.9
- gate_weight: bfloat16 [2048, 5632], P('fs', 'tp'), may hold values from -0.125 to 0.125
- up_weight: bfloat16 [2048, 5632], P('fs', 'tp'), may hold values from -0.125 to 0.125
- down_weight: bfloat16 [5632, 2048], P('tp', 'fs'), may hold values from -0.078125 to 0.078125
Outputs:
- mixed: bfloat16 [8192, 2048], P(('fs', 'tp'))
All inputs are finite; a program needn't handle non-finite values.
Results may differ from a plain program's by a relative error of at most 0.014.
Values may be sent and summed in bfloat16 or wider, within the bound.
A program may use at most 128 MiB of HBM per device.

v0:
```python
import functools

import jax
import jax.numpy as jnp
from jax import lax
from jax.experimental import pallas as pl
from jax.experimental.pallas import tpu as pltpu
from jax.sharding import PartitionSpec as P

MESH = pl.DeviceIdType.MESH
CORES = 2
GATE, UP, DOWN = 0, 1, 2


def fs_grid(n):
    ny = 1
    while ny * ny * 4 <= n:
        ny *= 2
    return n // ny, ny


def flip(v, bits):
    bit = 1
    while bit <= bits:
        if bits & bit:
            v = v + bit - 2 * bit * lax.rem(lax.div(v, bit), 2)
        bit *= 2
    return v


def block_order(nz, ny):
    order = [(0, 0)]
    for r in range(1, nz):
        order += [(r, 0)] + [(r - 1, s) for s in range(1, ny)]
    return order + [(nz - 1, s) for s in range(1, ny)]


def kernel(
    nz, ny, nx, tile, tok, gain, gw, uw, dw, out,
    xr, wg, wu, wd, ag, au, hid, pb, xv, sv, av, bv,
    own_sem, tok_sem, tok_recv, z_sem, y_sem, c_sem, w_recv, x_sem, x_recv, a_sem, a_recv, b_sem, b_recv,
):
    fs, tp = lax.axis_index("fs"), lax.axis_index("tp")
    z, y = lax.div(fs, ny), lax.rem(fs, ny)
    x, c = lax.div(tp, CORES), lax.rem(tp, CORES)
    near, other = flip(z, 1), 1 - c
    prim = c == lax.rem(z, 2)
    second = c != lax.rem(z, 2)
    count, width = xr.shape
    pieces, rp, ff = wg.shape[0], wg.shape[3], wg.shape[4]
    rows_in, wide = gw.shape[0], wd.shape[3]
    fp = ff // pieces
    part = count // nx
    half = part // 2
    keep = part // CORES

    def dev(z, y, x, c):
        return (z * ny + y, x * CORES + c)

    def send(src, dst, sent, got, where):
        pltpu.make_async_remote_copy(src_ref=src, dst_ref=dst, send_sem=sent, recv_sem=got, device_id=where, device_id_type=MESH).start()

    def wait(ref, sem):
        pltpu.make_async_copy(ref, ref, sem).wait()

    def slot(m, i, r, s):
        if m == DOWN:
            return wd.at[r, s, pl.ds(i * fp, fp)]
        return (wg, wu)[m].at[i, r, s]

    def mine(m, i):
        if m == DOWN:
            return dw.at[pl.ds(i * fp, fp)]
        return (gw, uw)[m].at[pl.ds(i * rp, rp)]

    def to_z(m, i, r):
        send(mine(m, i), slot(m, i, r, 0), z_sem.at[m, r], w_recv.at[m, i, r, 0], dev(flip(z, r), y, x, c))

    def to_y(m, i, r, src):
        for s in range(1, ny):
            send(src, slot(m, i, r, s), y_sem.at[m, s], w_recv.at[m, i, r, s], dev(z, flip(y, s), x, c))

    def to_core(m, i, r, s, src):
        send(src, slot(m, i, r, s), c_sem.at[m], w_recv.at[m, i, r, s], dev(z, y, x, other))

    def local(m, i):
        return pltpu.make_async_copy(mine(m, i), slot(m, i, 0, 0), own_sem.at[m, i])

    barrier = pltpu.get_barrier_semaphore()

    def greet(where):
        pl.semaphore_signal(barrier, inc=1, device_id=where, device_id_type=MESH)

    for r in range(1, nz):
        greet(dev(flip(z, r), y, x, c))
    for t in range(1, nx):
        greet(dev(z, y, flip(x, t), c))
    greet(dev(z, y, x, other))

    @pl.when(prim)
    def _():
        for s in range(1, ny):
            greet(dev(z, flip(y, s), x, c))
        pl.semaphore_wait(barrier, nz + nx + ny - 2)

    @pl.when(second)
    def _():
        greet(dev(near, y, x, other))
        pl.semaphore_wait(barrier, nz + nx)

    first = x * part

    @pl.when(prim)
    def _():
        rows = pl.ds(first, half)
        send(tok.at[rows], xr.at[rows], tok_sem.at[0], tok_recv.at[0, 0], dev(near, y, x, c))
        pltpu.make_async_copy(tok, xr, tok_sem.at[nx]).start()
        for m in (GATE, UP):
            for i in range(pieces):
                local(m, i).start()
        for i in range(pieces):
            for m in (GATE, UP):
                to_y(m, i, 0, mine(m, i))
                for r in range(2, nz, 2):
                    to_z(m, i, r)
        for m in (GATE, UP):
            for i in range(pieces):
                to_core(m, i, 0, 0, mine(m, i))
        for i in range(pieces):
            local(DOWN, i).start()
            to_core(DOWN, i, 0, 0, mine(DOWN, i))
        wait(xr, tok_sem.at[nx])

    @pl.when(second)
    def _():
        rows = pl.ds(first + half, half)
        send(tok.at[rows], xr.at[rows], tok_sem.at[0], tok_recv.at[1, 0], dev(near, y, x, other))
        for i in range(pieces):
            for r in range(1, nz, 2):
                for m in (GATE, UP):
                    to_z(m, i, r)
        for h in range(2):
            rows = pl.ds(first + h * half, half)
            wait(xr.at[rows], tok_recv.at[h, 0])
            for t in range(1, nx):
                send(xr.at[rows], xr.at[rows], tok_sem.at[t], tok_recv.at[h, t], dev(z, y, flip(x, t), c))
        for t in range(1, nx):
            for h in range(2):
                rows = pl.ds(flip(x, t) * part + h * half, half)
                wait(xr.at[rows], tok_recv.at[h, t])
            wait(xr.at[pl.ds(first, part)], tok_sem.at[t])

    def normalize(t, carry):
        rows = pl.ds(pl.multiple_of(t * 32, 32), 32)
        xf = xr[rows, :].astype(jnp.float32)
        scale = lax.rsqrt(jnp.mean(xf * xf, axis=-1, keepdims=True) + 1e-06)
        xr[rows, :] = (xf * scale * gain[...]).astype(jnp.bfloat16)
        return carry

    lax.fori_loop(0, count // 32, normalize, 0)

    def columns(i, r, s):
        at = (flip(z, r) * ny + flip(y, s)) * rows_in + i * rp
        return pl.ds(pl.multiple_of(at, rp), rp)

    def accumulate(i, pair, begin, end):
        rs = (2 * pair, 2 * pair + 1)

        def step(t, carry):
            rows = pl.ds(pl.multiple_of(t * tile, tile), tile)
            left = jnp.concatenate([xr[rows, columns(i, r, s)] for r in rs for s in range(ny)], axis=1)
            both = []
            for w, acc in ((wg, ag), (wu, au)):
                right = w[i, rs[0] : rs[1] + 1].reshape(2 * ny * rp, ff)
                total = jnp.dot(left, right, preferred_element_type=jnp.float32)
                if not begin:
                    total = acc[rows, :] + total
                if not end:
                    acc[rows, :] = total
                both.append(total)
            if end:
                g, u = both
                hid[rows, :] = (g / (1.0 + jnp.exp(-g)) * u).astype(jnp.bfloat16)
            return carry

        lax.fori_loop(0, count // tile, step, 0)

    def take(m, i, r, s):
        if (r, s) == (0, 0):

            @pl.when(prim)
            def _():
                local(m, i).wait()

            @pl.when(second)
            def _():
                wait(slot(m, i, r, s), w_recv.at[m, i, r, s])

        else:
            wait(slot(m, i, r, s), w_recv.at[m, i, r, s])

            @pl.when(prim)
            def _():
                if s == 0:
                    to_y(m, i, r, slot(m, i, r, s))
                to_core(m, i, r, s, slot(m, i, r, s))

    pairs = nz // 2
    for i in range(pieces):
        for pair in range(pairs):
            for s in range(ny):
                for r in (2 * pair, 2 * pair + 1):
                    for m in (GATE, UP):
                        take(m, i, r, s)
            end = i == pieces - 1 and pair == pairs - 1
            if end:

                @pl.when(prim)
                def _():
                    for k in range(pieces):
                        to_y(DOWN, k, 0, mine(DOWN, k))
                        for r in range(2, nz, 2):
                            to_z(DOWN, k, r)

                @pl.when(second)
                def _():
                    for k in range(pieces):
                        for r in range(1, nz, 2):
                            to_z(DOWN, k, r)

            accumulate(i, pair, i == 0 and pair == 0, end)

    order = block_order(nz, ny)

    def at(r, s):
        return r * ny + s

    def partial(r, s):
        j = at(r, s)
        for i in range(pieces):
            take(DOWN, i, r, s)

        def step(t, carry):
            rows = pl.ds(pl.multiple_of(t * tile, tile), tile)
            pb[j, rows, :] = jnp.dot(hid[rows, :], wd[r, s], preferred_element_type=jnp.float32).astype(jnp.bfloat16)
            return carry

        lax.fori_loop(0, count // tile, step, 0)
        for t in range(1, nx):
            there = flip(x, t)
            send(pb.at[j, pl.ds(there * part, part)], xv.at[t - 1, j], x_sem.at[t], x_recv.at[t, j], dev(z, y, there, c))

    def gather_x(r, s):
        j = at(r, s)
        total = pb[j, pl.ds(pl.multiple_of(x * part, part), part), :].astype(jnp.float32)
        for t in range(1, nx):
            wait(xv.at[t - 1, j], x_recv.at[t, j])
            total = total + xv[t - 1, j].astype(jnp.float32)
        sv[j] = total.astype(jnp.bfloat16)

        @pl.when(prim)
        def _():
            send(sv.at[j, pl.ds(other * keep, keep)], av.at[j], a_sem, a_recv.at[j], dev(z, y, x, other))

        @pl.when(second)
        def _():
            there = at(r ^ 1, s)
            for k in range(CORES):
                send(sv.at[j, pl.ds(k * keep, keep)], bv.at[there], b_sem.at[k], b_recv.at[there], dev(near, y, x, k))

    def finish(r, s):
        j = at(r, s)
        to = pl.ds(pl.multiple_of((flip(z, r) * ny + flip(y, s)) * wide, wide), wide)
        wait(bv.at[j], b_recv.at[j])

        @pl.when(prim)
        def _():
            a = sv[j, pl.ds(pl.multiple_of(c * keep, keep), keep), :].astype(jnp.float32)
            out[:, to] = (a + bv[j].astype(jnp.float32)).astype(jnp.bfloat16)

        @pl.when(second)
        def _():
            wait(av.at[j], a_recv.at[j])
            out[:, to] = (av[j].astype(jnp.float32) + bv[j].astype(jnp.float32)).astype(jnp.bfloat16)

    lag, late = 3, 6
    for n in range(len(order) + late):
        if n < len(order):
            partial(*order[n])
        if 0 <= n - lag < len(order):
            gather_x(*order[n - lag])
        if 0 <= n - late < len(order):
            finish(*order[n - late])

    wait(xr.at[pl.ds(0, half)], tok_sem.at[0])
    for t in range(1, nx):
        wait(xv.at[t - 1], x_sem.at[t])

    def block(m):
        return wd.at[0, 0] if m == DOWN else (wg, wu)[m].at[:, 0, 0]

    @pl.when(prim)
    def _():
        for m, whole, line in ((GATE, wg, wg.at[:, :, 0]), (UP, wu, wu.at[:, :, 0]), (DOWN, wd, wd.at[:, 0])):
            for r in range(2, nz, 2):
                wait(block(m), z_sem.at[m, r])
            for s in range(1, ny):
                wait(line, y_sem.at[m, s])
            wait(whole, c_sem.at[m])
        wait(av, a_sem)

    @pl.when(second)
    def _():
        for m in (GATE, UP, DOWN):
            for r in range(1, nz, 2):
                wait(block(m), z_sem.at[m, r])
        for k in range(CORES):
            wait(bv, b_sem.at[k])


def make_per_device(n, n_tp):
    nz, ny = fs_grid(n)
    nx = n_tp // CORES

    def per_device(tokens, norm_gain, gate_weight, up_weight, down_weight):
        count, width = tokens.shape
        rows, ff = gate_weight.shape
        wide = down_weight.shape[1]
        pieces = max(rows // 128, 1)
        keep = count // n_tp
        part = count // nx
        tile = min(256, count)
        bf16, f32 = jnp.bfloat16, jnp.float32
        dma = pltpu.SemaphoreType.DMA
        vmem = pl.BlockSpec(memory_space=pltpu.VMEM)
        hbm = pl.BlockSpec(memory_space=pl.ANY)
        return pl.pallas_call(
            functools.partial(kernel, nz, ny, nx, tile),
            name="gated_block",
            out_shape=jax.ShapeDtypeStruct((keep, width), bf16),
            in_specs=[hbm, vmem, hbm, hbm, hbm],
            out_specs=vmem,
            scratch_shapes=[
                pltpu.VMEM((count, width), bf16),
                pltpu.VMEM((pieces, nz, ny, rows // pieces, ff), bf16),
                pltpu.VMEM((pieces, nz, ny, rows // pieces, ff), bf16),
                pltpu.VMEM((nz, ny, ff, wide), bf16),
                pltpu.VMEM((count, ff), f32),
                pltpu.VMEM((count, ff), f32),
                pltpu.VMEM((count, ff), bf16),
                pltpu.VMEM((n, count, wide), bf16),
                pltpu.VMEM((nx - 1, n, part, wide), bf16),
                pltpu.VMEM((n, part, wide), bf16),
                pltpu.VMEM((n, keep, wide), bf16),
                pltpu.VMEM((n, keep, wide), bf16),
                dma((3, pieces)),
                dma((nx + 1,)),
                dma((2, nx)),
                dma((3, nz)),
                dma((3, ny)),
                dma((3,)),
                dma((3, pieces, nz, ny)),
                dma((nx,)),
                dma((nx, n)),
                dma,
                dma((n,)),
                dma((CORES,)),
                dma((n,)),
            ],
            compiler_params=pltpu.CompilerParams(collective_id=0, has_side_effects=True, vmem_limit_bytes=67043328),
        )(tokens, norm_gain.reshape(1, width), gate_weight, up_weight, down_weight)

    return per_device


def solution(mesh):
    placed = (P("fs", None), P(), P("fs", "tp"), P("fs", "tp"), P("tp", "fs"))
    return jax.shard_map(
        make_per_device(mesh.shape["fs"], mesh.shape["tp"]),
        mesh=mesh, in_specs=placed, out_specs=P(("fs", "tp"), None), check_vma=False,
    )
```

profile of v0, /device:TPU:1, one launch (start us, length us, event | category | flops | bytes accessed | tf_op | source)
XLA Modules:
  0.0 197.5 jit_solution(10082528924393325933)
XLA Ops:
  0.0 195.2 %gated_block.1 = bf16[256,2048]{1,0:T(8,128)(2,1)} custom-call(bf16[1024,2048]{1,0:T(8,128)(2,1)} %tok.1, f32[1,2048]{1,0:T(1,128)} %bitcast.1, bf16[256,1408]{1,0:T(8,128)(2,1)} %gw.1, bf16[256,1408]{1,0:T(8,128)(2,1)} %uw.1, bf16[1408,256]{1,0:T(8,128)(2,1)} %dw.1), custom_call_target="tpu_custom_call" | custom-call | tf_op jit(solution)/shard_map/gated_block/pallas_call | solution.py:337
  195.2 2.3 %copy.7 = bf16[256,2048]{1,0:T(8,128)(2,1)} copy(bf16[256,2048]{1,0:T(8,128)(2,1)} %gated_block.1) | data formatting | bytes 2097152
where the time goes:
time: 198 us; the launch traced here: 197 us
  Pallas kernels  195 us (98%)
  local copies, waits for them, and re-layouts  2.3 us (1%)
    pallas_call x1, Pallas kernels, per_device(): pl.pallas_call(functools.partial(kernel, nz, ny, nx, tile), name='gated_b...  195 us

commit v1 on v0

v1 whole, which is shorter than its diff:
```python
import functools

import jax
import jax.numpy as jnp
from jax import lax
from jax.experimental import pallas as pl
from jax.experimental.pallas import tpu as pltpu
from jax.sharding import PartitionSpec as P

MESH = pl.DeviceIdType.MESH
CORES = 2
GATE, UP, DOWN = 0, 1, 2


def fs_grid(n):
    ny = 1
    while ny * ny * 4 <= n:
        ny *= 2
    return n // ny, ny


def flip(v, bits):
    bit = 1
    while bit <= bits:
        if bits & bit:
            v = v + bit - 2 * bit * lax.rem(lax.div(v, bit), 2)
        bit *= 2
    return v


def inner(z):
    return lax.rem(lax.rem(z, 2) + lax.rem(lax.div(z, 2), 2), 2)


def swap_last(v, on):
    return v + on * (1 - 2 * lax.rem(v, 2))


def kernel(
    nz, ny, nx, tile, tok, gain, gw, uw, dw, out,
    xr, wg, wu, wd, ag, au, hid, pb, xv, sv, av, bv,
    own_sem, tok_sem, tok_recv, z_sem, y_sem, c_sem, w_recv, x_sem, x_recv, a_sem, a_recv, b_sem, b_recv,
):
    fs, tp = lax.axis_index("fs"), lax.axis_index("tp")
    z, y = lax.div(fs, ny), lax.rem(fs, ny)
    x, c = lax.div(tp, CORES), lax.rem(tp, CORES)
    near, other = flip(z, 1), 1 - c
    prim = c == lax.rem(z, 2)
    second = c != lax.rem(z, 2)
    count, width = xr.shape
    pieces, rp, ff = wg.shape[1], wg.shape[3], wg.shape[4]
    rows_in, wide = gw.shape[0], wd.shape[3]
    fp = ff // pieces
    part = count // nx
    chunks = tok_recv.shape[0]
    chunk = part // chunks
    keep = part // CORES
    scope = jax.named_scope

    def dev(z, y, x, c):
        return (z * ny + y, x * CORES + c)

    def send(src, dst, sent, got, where):
        pltpu.make_async_remote_copy(src_ref=src, dst_ref=dst, send_sem=sent, recv_sem=got, device_id=where, device_id_type=MESH).start()

    def wait(ref, sem):
        pltpu.make_async_copy(ref, ref, sem).wait()

    inside = inner(z)

    def pick(edge, middle):
        if isinstance(edge, int) and edge == middle:
            return edge
        return edge + inside * (middle - edge)

    def source(q):
        if isinstance(q, tuple):
            return pick(source(q[0]), source(q[1]))
        there = flip(z, q)
        return swap_last(there, inside) if q > 1 else there

    def number(v):
        return pick(*v) if isinstance(v, tuple) else v

    def slot(m, i, q, s):
        i, q = number(i), number(q)
        if m == DOWN:
            return wd.at[q, s, pl.ds(i * fp, fp)]
        return (wg, wu)[m].at[q, i, s]

    def mine(m, i):
        if m == DOWN:
            return dw.at[pl.ds(i * fp, fp)]
        return (gw, uw)[m].at[pl.ds(i * rp, rp)]

    def to_z(m, i, r):
        there = flip(z, r)
        q = r if r < 2 else swap_last(r, inner(there))
        send(mine(m, i), slot(m, i, q, 0), z_sem.at[m, r], w_recv.at[m, i, q, 0], dev(there, y, x, c))

    def to_y(m, i, q, src):
        for s in range(1, ny):
            send(src, slot(m, i, q, s), y_sem.at[m, s], w_recv.at[m, number(i), number(q), s], dev(z, flip(y, s), x, c))

    def to_core(m, i, q, s, src):
        send(src, slot(m, i, q, s), c_sem.at[m], w_recv.at[m, number(i), number(q), s], dev(z, y, x, other))

    def local(m, i):
        return pltpu.make_async_copy(mine(m, i), slot(m, i, 0, 0), own_sem.at[m, i])

    barrier = pltpu.get_barrier_semaphore()

    def greet(where):
        pl.semaphore_signal(barrier, inc=1, device_id=where, device_id_type=MESH)

    for r in range(1, nz):
        greet(dev(flip(z, r), y, x, c))
    for t in range(1, nx):
        greet(dev(z, y, flip(x, t), c))
    greet(dev(z, y, x, other))

    @pl.when(prim)
    def _():
        for s in range(1, ny):
            greet(dev(z, flip(y, s), x, c))
        pltpu.make_async_copy(tok, xr, tok_sem.at[nx]).start()
        for i in range(pieces):
            for m in (GATE, UP, DOWN):
                local(m, i).start()
        with scope("barrier"):
            pl.semaphore_wait(barrier, nz + nx + ny - 2)

    @pl.when(second)
    def _():
        greet(dev(near, y, x, other))
        with scope("barrier"):
            pl.semaphore_wait(barrier, nz + nx)

    def token_rows(x, k):
        return pl.ds(x * part + k * chunk, chunk)

    def to_near(k, core):
        rows = token_rows(x, k)
        send(tok.at[rows], xr.at[rows], tok_sem.at[0], tok_recv.at[k, 0], dev(near, y, x, core))

    @pl.when(prim)
    def _():
        for k in range(0, chunks, 2):
            to_near(k, c)
        for i in range(pieces):
            for m in (GATE, UP):
                to_y(m, i, 0, mine(m, i))
                for r in range(2, nz, 2):
                    to_z(m, i, r)
        for m in (GATE, UP, DOWN):
            for i in range(pieces):
                if m == DOWN:
                    to_y(m, i, 0, mine(m, i))
                to_core(m, i, 0, 0, mine(m, i))
        with scope("tokens"):
            wait(xr, tok_sem.at[nx])

    @pl.when(second)
    def _():
        for k in range(1, chunks, 2):
            to_near(k, other)
        for r in range(1, nz, 2):
            for i in range(pieces):
                for m in (GATE, UP):
                    to_z(m, i, r)

        @pl.when(inner(z) == 1)
        def _():
            for i in range(pieces):
                for r in range(3, nz, 2):
                    to_z(DOWN, i, r)

        for k in range(chunks):
            rows = token_rows(x, k)
            with scope(f"tokens#k={k}"):
                wait(xr.at[rows], tok_recv.at[k, 0])
            for t in range(1, nx):
                send(xr.at[rows], xr.at[rows], tok_sem.at[t], tok_recv.at[k, t], dev(z, y, flip(x, t), c))
        with scope("tokens#x"):
            for t in range(1, nx):
                for k in range(chunks):
                    rows = token_rows(flip(x, t), k)
                    wait(xr.at[rows], tok_recv.at[k, t])
                wait(xr.at[pl.ds(x * part, part)], tok_sem.at[t])

    def normalize(t, carry):
        rows = pl.ds(pl.multiple_of(t * 32, 32), 32)
        xf = xr[rows, :].astype(jnp.float32)
        scale = lax.rsqrt(jnp.mean(xf * xf, axis=-1, keepdims=True) + 1e-06)
        xr[rows, :] = (xf * scale * gain[...]).astype(jnp.bfloat16)
        return carry

    with scope("normalize"):
        lax.fori_loop(0, count // 32, normalize, 0)

    def columns(q, i, s):
        at = (source(q) * ny + flip(y, s)) * rows_in + number(i) * rp
        return pl.ds(pl.multiple_of(at, rp), rp)

    def accumulate(group, begin=False, end=False):
        def step(t, carry):
            rows = pl.ds(pl.multiple_of(t * tile, tile), tile)
            left = jnp.concatenate([xr[rows, columns(q, i, s)] for q, i in group for s in range(ny)], axis=1)
            both = []
            for w, acc in ((wg, ag), (wu, au)):
                right = jnp.concatenate([w[number(q), number(i)].reshape(ny * rp, ff) for q, i in group], axis=0)
                total = jnp.dot(left, right, preferred_element_type=jnp.float32)
                if not begin:
                    total = acc[rows, :] + total
                if not end:
                    acc[rows, :] = total
                both.append(total)
            if end:
                g, u = both
                hid[rows, :] = (g / (1.0 + jnp.exp(-g)) * u).astype(jnp.bfloat16)
            return carry

        with scope("acc#" + "#".join(f"{q}={i}" for q, i in group)):
            lax.fori_loop(0, count // tile, step, 0)

    def take(m, i, q, s):
        if (q, s) == (0, 0):

            @pl.when(prim)
            def _():
                local(m, i).wait()

            @pl.when(second)
            def _():
                wait(slot(m, i, q, s), w_recv.at[m, number(i), number(q), s])

        else:
            with scope(f"take#m={m}#i={i}#q={q}#s={s}".replace(" ", "")):
                wait(slot(m, i, q, s), w_recv.at[m, number(i), number(q), s])

            @pl.when(prim)
            def _():
                if s == 0:
                    to_y(m, i, q, slot(m, i, q, s))
                to_core(m, i, q, s, slot(m, i, q, s))

    def take_both(i, q, rows):
        for s in rows:
            for m in (GATE, UP):
                take(m, i, q, s)

    def take_down(q, rows):
        for s in rows:
            for i in range(pieces):
                take(DOWN, i, q, s)

    here, away = range(1), range(1, ny)
    early, late = list(range(2, nz, 2)), [1] + list(range(3, nz, 2))
    every = range(pieces)
    for i in every:
        take_both(i, 0, range(ny))
    accumulate([(0, i) for i in every], begin=True)
    steps = [
        ((q0, q1), (i0, i1))
        for (q0, i0), (q1, i1) in zip([(q, i) for q in late for i in every], [(q, i) for i in every for q in late])
    ]

    def pass_on(n):
        if n < len(steps):
            q, i = steps[n]
            take_both(i, q, here)

    def down_to_z():
        @pl.when(prim)
        def _():
            for k in every:
                for r in range(2, nz, 2):
                    to_z(DOWN, k, r)

        @pl.when(second)
        def _():
            for k in every:
                to_z(DOWN, k, 1)

            @pl.when(inside == 0)
            def _():
                for k in every:
                    for r in range(3, nz, 2):
                        to_z(DOWN, k, r)

    for q in early:
        for i in every:
            take_both(i, q, here)
    pass_on(0)
    for q in early:
        for i in every:
            take_both(i, q, away)
    pass_on(1)
    for q in early:
        accumulate([(q, k) for k in every])
    pass_on(2)
    group = []
    for n, (q, i) in enumerate(steps):
        last = n == len(steps) - 1
        take_both(i, q, away)
        pass_on(n + 3)
        if n + 4 == max(len(steps), 4):
            down_to_z()
        group.append((q, i))
        if last or n == len(steps) - 2 or n % 2:
            accumulate(group, end=last)
            group = []

    def at(q, s):
        return q * ny + s

    def partial(q, s):
        j = at(q, s)

        def step(t, carry):
            rows = pl.ds(pl.multiple_of(t * tile, tile), tile)
            pb[j, rows, :] = jnp.dot(hid[rows, :], wd[q, s], preferred_element_type=jnp.float32).astype(jnp.bfloat16)
            return carry

        with scope(f"part#q={q}#s={s}"):
            lax.fori_loop(0, count // tile, step, 0)
        for t in range(1, nx):
            there = flip(x, t)
            send(pb.at[j, pl.ds(there * part, part)], xv.at[t - 1, j], x_sem.at[t], x_recv.at[t, j], dev(z, y, there, c))

    def gather_x(q, s):
        j = at(q, s)
        total = pb[j, pl.ds(pl.multiple_of(x * part, part), part), :].astype(jnp.float32)
        for t in range(1, nx):
            with scope(f"xwait#q={q}#s={s}"):
                wait(xv.at[t - 1, j], x_recv.at[t, j])
            total = total + xv[t - 1, j].astype(jnp.float32)
        sv[j] = total.astype(jnp.bfloat16)

        @pl.when(prim)
        def _():
            send(sv.at[j, pl.ds(other * keep, keep)], av.at[j], a_sem, a_recv.at[j], dev(z, y, x, other))

        @pl.when(second)
        def _():
            there = at(1 - q if q < 2 else q, s)
            for k in range(CORES):
                send(sv.at[j, pl.ds(k * keep, keep)], bv.at[there], b_sem.at[k], b_recv.at[there], dev(near, y, x, k))

    def finish(q, s):
        j = at(q, s)
        to = pl.ds(pl.multiple_of((source(q) * ny + flip(y, s)) * wide, wide), wide)
        with scope(f"bwait#q={q}#s={s}"):
            wait(bv.at[j], b_recv.at[j])

        @pl.when(prim)
        def _():
            a = sv[j, pl.ds(pl.multiple_of(c * keep, keep), keep), :].astype(jnp.float32)
            out[:, to] = (a + bv[j].astype(jnp.float32)).astype(jnp.bfloat16)

        @pl.when(second)
        def _():
            wait(av.at[j], a_recv.at[j])
            out[:, to] = (av[j].astype(jnp.float32) + bv[j].astype(jnp.float32)).astype(jnp.bfloat16)

    order = [(0, s) for s in range(ny)]
    for q in early:
        order += [(q, 0), (1, 0)] if q == 2 else [(q, 0)]
    if not early:
        order += [(1, 0)]
    for q in early:
        order += [(q, s) for s in away] + ([(1, s) for s in away] if q == 2 else [])
    if not early:
        order += [(1, s) for s in away]
    for q in late[1:]:
        order += [(q, 0)]
    for q in late[1:]:
        order += [(q, s) for s in away]
    ahead, lag, behind = 1, 3, 5
    finishes = {}
    for n, (q, s) in enumerate(order):
        n = max(n, order.index((1 - q if q < 2 else q, s)))
        finishes.setdefault(n + behind, []).append((q, s))
    for n in range(-ahead, len(order) + behind):
        if n + ahead < len(order):
            q, s = order[n + ahead]
            take_down(q, range(s, s + 1))
        if 0 <= n < len(order):
            partial(*order[n])
        if 0 <= n - lag < len(order):
            gather_x(*order[n - lag])
        for q, s in finishes.get(n, ()):
            finish(q, s)

    wait(xr.at[pl.ds(0, part // 2)], tok_sem.at[0])
    for t in range(1, nx):
        wait(xv.at[t - 1], x_sem.at[t])

    def block(m):
        return wd.at[0, 0] if m == DOWN else (wg, wu)[m].at[0, :, 0]

    @pl.when(prim)
    def _():
        for m, whole, line in ((GATE, wg, wg.at[:, :, 0]), (UP, wu, wu.at[:, :, 0]), (DOWN, wd, wd.at[:, 0])):
            for r in range(2, nz, 2):
                wait(block(m), z_sem.at[m, r])
            for s in range(1, ny):
                wait(line, y_sem.at[m, s])
            wait(whole, c_sem.at[m])
        wait(av, a_sem)

    @pl.when(second)
    def _():
        for m in (GATE, UP, DOWN):
            for r in range(1, nz, 2):
                wait(block(m), z_sem.at[m, r])
        for k in range(CORES):
            wait(bv, b_sem.at[k])


def make_per_device(n, n_tp):
    nz, ny = fs_grid(n)
    nx = n_tp // CORES

    def per_device(tokens, norm_gain, gate_weight, up_weight, down_weight):
        count, width = tokens.shape
        rows, ff = gate_weight.shape
        wide = down_weight.shape[1]
        pieces = max(rows // 128, 1)
        keep = count // n_tp
        part = count // nx
        chunks = 8
        tile = min(256, count)
        bf16, f32 = jnp.bfloat16, jnp.float32
        dma = pltpu.SemaphoreType.DMA
        vmem = pl.BlockSpec(memory_space=pltpu.VMEM)
        hbm = pl.BlockSpec(memory_space=pl.ANY)
        return pl.pallas_call(
            functools.partial(kernel, nz, ny, nx, tile),
            name="gated_block",
            out_shape=jax.ShapeDtypeStruct((keep, width), bf16),
            in_specs=[hbm, vmem, hbm, hbm, hbm],
            out_specs=vmem,
            scratch_shapes=[
                pltpu.VMEM((count, width), bf16),
                pltpu.VMEM((nz, pieces, ny, rows // pieces, ff), bf16),
                pltpu.VMEM((nz, pieces, ny, rows // pieces, ff), bf16),
                pltpu.VMEM((nz, ny, ff, wide), bf16),
                pltpu.VMEM((count, ff), f32),
                pltpu.VMEM((count, ff), f32),
                pltpu.VMEM((count, ff), bf16),
                pltpu.VMEM((n, count, wide), bf16),
                pltpu.VMEM((nx - 1, n, part, wide), bf16),
                pltpu.VMEM((n, part, wide), bf16),
                pltpu.VMEM((n, keep, wide), bf16),
                pltpu.VMEM((n, keep, wide), bf16),
                dma((3, pieces)),
                dma((nx + 1,)),
                dma((chunks, nx)),
                dma((3, nz)),
                dma((3, ny)),
                dma((3,)),
                dma((3, pieces, nz, ny)),
                dma((nx,)),
                dma((nx, n)),
                dma,
                dma((n,)),
                dma((CORES,)),
                dma((n,)),
            ],
            compiler_params=pltpu.CompilerParams(collective_id=0, has_side_effects=True, vmem_limit_bytes=67043328),
        )(tokens, norm_gain.reshape(1, width), gate_weight, up_weight, down_weight)

    return per_device


def solution(mesh):
    placed = (P("fs", None), P(), P("fs", "tp"), P("fs", "tp"), P("tp", "fs"))
    return jax.shard_map(
        make_per_device(mesh.shape["fs"], mesh.shape["tp"]),
        mesh=mesh, in_specs=placed, out_specs=P(("fs", "tp"), None), check_vma=False,
    )
```

time: 198 us -> 147 us (0.74)
  Pallas kernels: 195 us -> 145 us
    pallas_call x1, Pallas kernels: 195 us -> 145 us  [per_device(): pl.pallas_call(functools.partial(kernel, nz, ny, nx, tile), name='gated_b...]
where the time goes in v1:
time: 147 us
  Pallas kernels  145 us (99%)
  local copies, waits for them, and re-layouts  2.3 us (2%)
    pallas_call x1, Pallas kernels, per_device(): pl.pallas_call(functools.partial(kernel, nz, ny, nx, tile), name='gated_b...  145 us

profile of v1, /device:TPU:1, one launch (start us, length us, event | category | flops | bytes accessed | tf_op | source)
XLA Modules:
  0.0 146.9 jit_solution(1206984640042054304)
XLA Ops:
  0.0 144.6 %gated_block.1 = bf16[256,2048]{1,0:T(8,128)(2,1)} custom-call(bf16[1024,2048]{1,0:T(8,128)(2,1)} %tok.1, f32[1,2048]{1,0:T(1,128)} %bitcast.1, bf16[256,1408]{1,0:T(8,128)(2,1)} %gw.1, bf16[256,1408]{1,0:T(8,128)(2,1)} %uw.1, bf16[1408,256]{1,0:T(8,128)(2,1)} %dw.1), custom_call_target="tpu_custom_call" | custom-call | tf_op jit(solution)/shard_map/gated_block/pallas_call | solution.py:438
  144.6 2.3 %copy.7 = bf16[256,2048]{1,0:T(8,128)(2,1)} copy(bf16[256,2048]{1,0:T(8,128)(2,1)} %gated_block.1) | data formatting | bytes 2097152

commit v2 on v1

--- a/solution.py
+++ b/solution.py
@@ -38,8 +38,8 @@
 
 def kernel(
     nz, ny, nx, tile, tok, gain, gw, uw, dw, out,
-    xr, wg, wu, wd, ag, au, hid, pb, xv, sv, av, bv,
-    own_sem, tok_sem, tok_recv, z_sem, y_sem, c_sem, w_recv, x_sem, x_recv, a_sem, a_recv, b_sem, b_recv,
+    xr, wg, wu, wd, ag, au, hid, pb, xv, sv, av, bv, zv, ob,
+    own_sem, tok_sem, tok_recv, z_sem, y_sem, c_sem, w_recv, x_sem, x_recv, a_sem, a_recv, b_sem, b_recv, zv_sem, zv_recv, out_sem,
 ):
     fs, tp = lax.axis_index("fs"), lax.axis_index("tp")
     z, y = lax.div(fs, ny), lax.rem(fs, ny)
@@ -169,11 +169,17 @@
                 for m in (GATE, UP):
                     to_z(m, i, r)
 
-        @pl.when(inner(z) == 1)
+        for r in range(3, nz, 2):
+            for i in range(pieces):
+
+                @pl.when(inside == 1)
+                def _():
+                    to_z(DOWN, i, r)
+
+        @pl.when(inside == 0)
         def _():
             for i in range(pieces):
-                for r in range(3, nz, 2):
-                    to_z(DOWN, i, r)
+                to_z(DOWN, i, 1)
 
         for k in range(chunks):
             rows = token_rows(x, k)
@@ -202,9 +208,9 @@
         at = (source(q) * ny + flip(y, s)) * rows_in + number(i) * rp
         return pl.ds(pl.multiple_of(at, rp), rp)
 
-    def accumulate(group, begin=False, end=False):
+    def accumulate(group, begin=False, end=False, start=0, span=None):
         def step(t, carry):
-            rows = pl.ds(pl.multiple_of(t * tile, tile), tile)
+            rows = pl.ds(pl.multiple_of(start + t * tile, tile), tile)
             left = jnp.concatenate([xr[rows, columns(q, i, s)] for q, i in group for s in range(ny)], axis=1)
             both = []
             for w, acc in ((wg, ag), (wu, au)):
@@ -221,7 +227,7 @@
             return carry
 
         with scope("acc#" + "#".join(f"{q}={i}" for q, i in group)):
-            lax.fori_loop(0, count // tile, step, 0)
+            lax.fori_loop(0, (span or count) // tile, step, 0)
 
     def take(m, i, q, s):
         if (q, s) == (0, 0):
@@ -270,23 +276,18 @@
             q, i = steps[n]
             take_both(i, q, here)
 
-    def down_to_z():
-        @pl.when(prim)
+    def down_to_z(place):
+        @pl.when(prim & (inside == place))
         def _():
             for k in every:
                 for r in range(2, nz, 2):
                     to_z(DOWN, k, r)
 
-        @pl.when(second)
+        @pl.when(second & (inside == place))
         def _():
             for k in every:
-                to_z(DOWN, k, 1)
-
-            @pl.when(inside == 0)
-            def _():
-                for k in every:
-                    for r in range(3, nz, 2):
-                        to_z(DOWN, k, r)
+                for r in [1] if place else range(3, nz, 2):
+                    to_z(DOWN, k, r)
 
     for q in early:
         for i in every:
@@ -302,99 +303,162 @@
     group = []
     for n, (q, i) in enumerate(steps):
         last = n == len(steps) - 1
+        if last:
+            down_to_z(0)
         take_both(i, q, away)
         pass_on(n + 3)
         if n + 4 == max(len(steps), 4):
-            down_to_z()
+            down_to_z(1)
         group.append((q, i))
-        if last or n == len(steps) - 2 or n % 2:
-            accumulate(group, end=last)
+        if not last and (n == len(steps) - 2 or n % 2):
+            accumulate(group)
             group = []
 
     def at(q, s):
         return q * ny + s
 
-    def partial(q, s):
+    parts = [flip(x, t) for t in range(1, nx)] + [x]
+    subs = (other, c)
+    straight = early[:1]
+
+    def sub_rows(x, k):
+        return pl.ds(pl.multiple_of(x * part + k * keep, keep), keep)
+
+    def to_x(j, t):
+        there = flip(x, t)
+        for h, k in enumerate(subs):
+            send(pb.at[j, sub_rows(there, k)], xv.at[t - 1, j, h], x_sem.at[t], x_recv.at[t, j, h], dev(z, y, there, c))
+
+    def partial(q, s, head=None):
         j = at(q, s)
-
-        def step(t, carry):
-            rows = pl.ds(pl.multiple_of(t * tile, tile), tile)
-            pb[j, rows, :] = jnp.dot(hid[rows, :], wd[q, s], preferred_element_type=jnp.float32).astype(jnp.bfloat16)
-            return carry
-
-        with scope(f"part#q={q}#s={s}"):
-            lax.fori_loop(0, count // tile, step, 0)
+        for t, p in enumerate(parts):
+            start = p * part
+            if head:
+                head(start)
+
+            def step(t, carry):
+                rows = pl.ds(pl.multiple_of(start + t * tile, tile), tile)
+                pb[j, rows, :] = jnp.dot(hid[rows, :], wd[q, s], preferred_element_type=jnp.float32).astype(jnp.bfloat16)
+                return carry
+
+            with scope(f"part#q={q}#s={s}"):
+                lax.fori_loop(0, part // tile, step, 0)
+            if q not in straight and t + 1 < nx:
+                to_x(j, t + 1)
+            if q in straight:
+
+                @pl.when(second)
+                def _():
+                    rows = pl.ds(pl.multiple_of(start, part), part)
+                    send(pb.at[j, rows], zv.at[s, rows], zv_sem, zv_recv.at[s, t], dev(near, y, x, c))
+
+    def gather_z(q, s):
+        j = at(q, s)
+
+        @pl.when(prim)
+        def _():
+            for t, p in enumerate(parts):
+                rows = pl.ds(pl.multiple_of(p * part, part), part)
+                with scope(f"zwait#q={q}#s={s}"):
+                    wait(zv.at[s, rows], zv_recv.at[s, t])
+                pb[j, rows, :] = (pb[j, rows, :].astype(jnp.float32) + zv[s, rows, :].astype(jnp.float32)).astype(jnp.bfloat16)
+                if t + 1 < nx:
+                    to_x(j, t + 1)
+
+    def added(j, h, k):
+        total = pb[j, sub_rows(x, k), :].astype(jnp.float32)
         for t in range(1, nx):
-            there = flip(x, t)
-            send(pb.at[j, pl.ds(there * part, part)], xv.at[t - 1, j], x_sem.at[t], x_recv.at[t, j], dev(z, y, there, c))
+            with scope(f"xwait#j={j}"):
+                wait(xv.at[t - 1, j, h], x_recv.at[t, j, h])
+            total = total + xv[t - 1, j, h].astype(jnp.float32)
+        return total.astype(jnp.bfloat16)
 
     def gather_x(q, s):
         j = at(q, s)
-        total = pb[j, pl.ds(pl.multiple_of(x * part, part), part), :].astype(jnp.float32)
-        for t in range(1, nx):
-            with scope(f"xwait#q={q}#s={s}"):
-                wait(xv.at[t - 1, j], x_recv.at[t, j])
-            total = total + xv[t - 1, j].astype(jnp.float32)
-        sv[j] = total.astype(jnp.bfloat16)
-
-        @pl.when(prim)
-        def _():
-            send(sv.at[j, pl.ds(other * keep, keep)], av.at[j], a_sem, a_recv.at[j], dev(z, y, x, other))
-
-        @pl.when(second)
-        def _():
-            there = at(1 - q if q < 2 else q, s)
-            for k in range(CORES):
-                send(sv.at[j, pl.ds(k * keep, keep)], bv.at[there], b_sem.at[k], b_recv.at[there], dev(near, y, x, k))
+        if q in straight:
+
+            @pl.when(prim)
+            def _():
+                for h, k in enumerate(subs):
+                    sv[j, h] = added(j, h, k)
+                    if h == 0:
+                        send(sv.at[j, h], av.at[j], a_sem, a_recv.at[j], dev(z, y, x, other))
+
+            return
+        there = at(1 - q if q < 2 else q, s)
+        for h, k in enumerate(subs):
+            sv[j, h] = added(j, h, k)
+            if h == 0:
+
+                @pl.when(prim)
+                def _():
+                    send(sv.at[j, h], av.at[j], a_sem, a_recv.at[j], dev(z, y, x, other))
+
+            @pl.when(second)
+            def _():
+                send(sv.at[j, h], bv.at[there], b_sem.at[h], b_recv.at[there], dev(near, y, x, k))
 
     def finish(q, s):
         j = at(q, s)
         to = pl.ds(pl.multiple_of((source(q) * ny + flip(y, s)) * wide, wide), wide)
-        with scope(f"bwait#q={q}#s={s}"):
-            wait(bv.at[j], b_recv.at[j])
+        if q not in straight:
+            with scope(f"bwait#q={q}#s={s}"):
+                wait(bv.at[j], b_recv.at[j])
+
+        def put(value):
+            if q not in straight:
+                value = (value.astype(jnp.float32) + bv[j].astype(jnp.float32)).astype(jnp.bfloat16)
+            ob[j] = value
 
         @pl.when(prim)
         def _():
-            a = sv[j, pl.ds(pl.multiple_of(c * keep, keep), keep), :].astype(jnp.float32)
-            out[:, to] = (a + bv[j].astype(jnp.float32)).astype(jnp.bfloat16)
+            put(sv[j, 1])
 
         @pl.when(second)
         def _():
             wait(av.at[j], a_recv.at[j])
-            out[:, to] = (av[j].astype(jnp.float32) + bv[j].astype(jnp.float32)).astype(jnp.bfloat16)
+            put(av[j])
+
+        pltpu.make_async_copy(ob.at[j], out.at[:, to], out_sem).start()
 
     order = [(0, s) for s in range(ny)]
-    for q in early:
-        order += [(q, 0), (1, 0)] if q == 2 else [(q, 0)]
-    if not early:
-        order += [(1, 0)]
-    for q in early:
-        order += [(q, s) for s in away] + ([(1, s) for s in away] if q == 2 else [])
-    if not early:
-        order += [(1, s) for s in away]
-    for q in late[1:]:
-        order += [(q, 0)]
-    for q in late[1:]:
-        order += [(q, s) for s in away]
-    ahead, lag, behind = 1, 3, 5
-    finishes = {}
+    order += [(q, 0) for q in early[:1]] + [(1, 0)]
+    order += [(q, s) for q in early[:1] for s in away]
+    order += [(q, 0) for q in late[1:] + early[1:]]
+    order += [(q, s) for q in late + early[1:] for s in away]
+    ahead = {1: [(q, 0) for q in early[:1]], ny: [(1, 0)]}
+    if early:
+        ahead[order.index((early[0], ny - 1)) + 1] = [(q, 0) for q in late[1:]]
+    taken = []
+    lag, behind = 3, 5
+    finishes, sums, adds = {}, {}, {}
     for n, (q, s) in enumerate(order):
+        extra = 0
+        if q in straight:
+            sums.setdefault(n + 3, []).append((q, s))
+            extra = 2
+        adds.setdefault(n + lag + extra, []).append((q, s))
         n = max(n, order.index((1 - q if q < 2 else q, s)))
         finishes.setdefault(n + behind, []).append((q, s))
-    for n in range(-ahead, len(order) + behind):
-        if n + ahead < len(order):
-            q, s = order[n + ahead]
-            take_down(q, range(s, s + 1))
-        if 0 <= n < len(order):
+    for n in range(len(order) + behind):
+        for q, s in sums.get(n, ()):
+            gather_z(q, s)
+        for q, s in ahead.get(n, []) + order[n : n + 1]:
+            if (q, s) not in taken:
+                taken.append((q, s))
+                take_down(q, range(s, s + 1))
+        if n == 0:
+            partial(*order[0], head=lambda start: accumulate(group, end=True, start=start, span=part))
+        elif 0 < n < len(order):
             partial(*order[n])
-        if 0 <= n - lag < len(order):
-            gather_x(*order[n - lag])
+        for q, s in adds.get(n, ()):
+            gather_x(q, s)
         for q, s in finishes.get(n, ()):
             finish(q, s)
 
+    wait(ob, out_sem)
     wait(xr.at[pl.ds(0, part // 2)], tok_sem.at[0])
-    for t in range(1, nx):
-        wait(xv.at[t - 1], x_sem.at[t])
+    n_across = xv.shape[1] - ny * len(straight)
 
     def block(m):
         return wd.at[0, 0] if m == DOWN else (wg, wu)[m].at[0, :, 0]
@@ -407,6 +471,8 @@
             for s in range(1, ny):
                 wait(line, y_sem.at[m, s])
             wait(whole, c_sem.at[m])
+        for t in range(1, nx):
+            wait(xv.at[t - 1], x_sem.at[t])
         wait(av, a_sem)
 
     @pl.when(second)
@@ -414,8 +480,12 @@
         for m in (GATE, UP, DOWN):
             for r in range(1, nz, 2):
                 wait(block(m), z_sem.at[m, r])
+        for t in range(1, nx):
+            wait(xv.at[t - 1, pl.ds(0, n_across)], x_sem.at[t])
         for k in range(CORES):
-            wait(bv, b_sem.at[k])
+            wait(bv.at[pl.ds(0, n_across)], b_sem.at[k])
+        if straight:
+            wait(zv, zv_sem)
 
 
 def make_per_device(n, n_tp):
@@ -440,7 +510,7 @@
             name="gated_block",
             out_shape=jax.ShapeDtypeStruct((keep, width), bf16),
             in_specs=[hbm, vmem, hbm, hbm, hbm],
-            out_specs=vmem,
+            out_specs=hbm,
             scratch_shapes=[
                 pltpu.VMEM((count, width), bf16),
                 pltpu.VMEM((nz, pieces, ny, rows // pieces, ff), bf16),
@@ -450,9 +520,11 @@
                 pltpu.VMEM((count, ff), f32),
                 pltpu.VMEM((count, ff), bf16),
                 pltpu.VMEM((n, count, wide), bf16),
-                pltpu.VMEM((nx - 1, n, part, wide), bf16),
-                pltpu.VMEM((n, part, wide), bf16),
+                pltpu.VMEM((nx - 1, n, CORES, keep, wide), bf16),
+                pltpu.VMEM((n, CORES, keep, wide), bf16),
                 pltpu.VMEM((n, keep, wide), bf16),
+                pltpu.VMEM((n, keep, wide), bf16),
+                pltpu.VMEM((ny, count, wide), bf16),
                 pltpu.VMEM((n, keep, wide), bf16),
                 dma((3, pieces)),
                 dma((nx + 1,)),
@@ -462,11 +534,14 @@
                 dma((3,)),
                 dma((3, pieces, nz, ny)),
                 dma((nx,)),
-                dma((nx, n)),
+                dma((nx, n, CORES)),
                 dma,
                 dma((n,)),
                 dma((CORES,)),
                 dma((n,)),
+                dma,
+                dma((ny, nx)),
+                dma,
             ],
             compiler_params=pltpu.CompilerParams(collective_id=0, has_side_effects=True, vmem_limit_bytes=67043328),
         )(tokens, norm_gain.reshape(1, width), gate_weight, up_weight, down_weight)

time: 147 us -> 138 us (0.939); the launches traced: 147 us -> 135 us
  Pallas kernels: 145 us -> 133 us
    pallas_call x1, Pallas kernels: 145 us -> 133 us  [per_device(): pl.pallas_call(functools.partial(kernel, nz, ny, nx, tile), name='gated_b...]
where the time goes in v2:
time: 138 us; the launch traced here: 135 us
  Pallas kernels  133 us (96%)
  local copies, waits for them, and re-layouts  2.3 us (2%)
    pallas_call x1, Pallas kernels, per_device(): pl.pallas_call(functools.partial(kernel, nz, ny, nx, tile), name='gated_b...  133 us

profile of v2, /device:TPU:1, one launch (start us, length us, event | category | flops | bytes accessed | tf_op | source)
XLA Modules:
  0.0 135.5 jit_solution(3242834890903530100)
XLA Ops:
  0.0 133.2 %gated_block.1 = bf16[256,2048]{1,0:T(8,128)(2,1)} custom-call(bf16[1024,2048]{1,0:T(8,128)(2,1)} %tok.1, f32[1,2048]{1,0:T(1,128)} %bitcast.1, bf16[256,1408]{1,0:T(8,128)(2,1)} %gw.1, bf16[256,1408]{1,0:T(8,128)(2,1)} %uw.1, bf16[1408,256]{1,0:T(8,128)(2,1)} %dw.1), custom_call_target="tpu_custom_call" | custom-call | tf_op jit(solution)/shard_map/gated_block/pallas_call | solution.py:508
  133.2 2.3 %copy.7 = bf16[256,2048]{1,0:T(8,128)(2,1)} copy(bf16[256,2048]{1,0:T(8,128)(2,1)} %gated_block.1) | data formatting | bytes 2097152

commit v3 on v2

--- a/solution.py
+++ b/solution.py
@@ -82,31 +82,40 @@
     def number(v):
         return pick(*v) if isinstance(v, tuple) else v
 
-    def slot(m, i, q, s):
+    cuts = w_recv.shape[4]
+    cut = rp // cuts
+
+    def slot(m, i, q, s, h):
         i, q = number(i), number(q)
         if m == DOWN:
             return wd.at[q, s, pl.ds(i * fp, fp)]
-        return (wg, wu)[m].at[q, i, s]
-
-    def mine(m, i):
+        return (wg, wu)[m].at[q, i, s, pl.ds(h * cut, cut)]
+
+    def mine(m, i, h):
         if m == DOWN:
             return dw.at[pl.ds(i * fp, fp)]
-        return (gw, uw)[m].at[pl.ds(i * rp, rp)]
+        return (gw, uw)[m].at[pl.ds(i * rp + h * cut, cut)]
+
+    def halves(m):
+        return range(1 if m == DOWN else cuts)
 
     def to_z(m, i, r):
         there = flip(z, r)
         q = r if r < 2 else swap_last(r, inner(there))
-        send(mine(m, i), slot(m, i, q, 0), z_sem.at[m, r], w_recv.at[m, i, q, 0], dev(there, y, x, c))
-
-    def to_y(m, i, q, src):
+        for h in halves(m):
+            send(mine(m, i, h), slot(m, i, q, 0, h), z_sem.at[m, r], w_recv.at[m, i, q, 0, h], dev(there, y, x, c))
+
+    def to_y(m, i, q, h, src):
         for s in range(1, ny):
-            send(src, slot(m, i, q, s), y_sem.at[m, s], w_recv.at[m, number(i), number(q), s], dev(z, flip(y, s), x, c))
-
-    def to_core(m, i, q, s, src):
-        send(src, slot(m, i, q, s), c_sem.at[m], w_recv.at[m, number(i), number(q), s], dev(z, y, x, other))
-
-    def local(m, i):
-        return pltpu.make_async_copy(mine(m, i), slot(m, i, 0, 0), own_sem.at[m, i])
+            got = w_recv.at[m, number(i), number(q), s, h]
+            send(src, slot(m, i, q, s, h), y_sem.at[m, s], got, dev(z, flip(y, s), x, c))
+
+    def to_core(m, i, q, s, h, src):
+        got = w_recv.at[m, number(i), number(q), s, h]
+        send(src, slot(m, i, q, s, h), c_sem.at[m], got, dev(z, y, x, other))
+
+    def local(m, i, h):
+        return pltpu.make_async_copy(mine(m, i, h), slot(m, i, 0, 0, h), own_sem.at[m, i, h])
 
     barrier = pltpu.get_barrier_semaphore()
 
@@ -126,7 +135,8 @@
         pltpu.make_async_copy(tok, xr, tok_sem.at[nx]).start()
         for i in range(pieces):
             for m in (GATE, UP, DOWN):
-                local(m, i).start()
+                for h in halves(m):
+                    local(m, i, h).start()
         with scope("barrier"):
             pl.semaphore_wait(barrier, nz + nx + ny - 2)
 
@@ -149,23 +159,27 @@
             to_near(k, c)
         for i in range(pieces):
             for m in (GATE, UP):
-                to_y(m, i, 0, mine(m, i))
+                for h in halves(m):
+                    to_y(m, i, 0, h, mine(m, i, h))
                 for r in range(2, nz, 2):
                     to_z(m, i, r)
         for m in (GATE, UP, DOWN):
             for i in range(pieces):
-                if m == DOWN:
-                    to_y(m, i, 0, mine(m, i))
-                to_core(m, i, 0, 0, mine(m, i))
+                for h in halves(m):
+                    if m == DOWN:
+                        to_y(m, i, 0, h, mine(m, i, h))
+                    to_core(m, i, 0, 0, h, mine(m, i, h))
         with scope("tokens"):
             wait(xr, tok_sem.at[nx])
 
     @pl.when(second)
     def _():
+        to_z(GATE, 0, 1)
+        to_z(UP, 0, 1)
         for k in range(1, chunks, 2):
             to_near(k, other)
         for r in range(1, nz, 2):
-            for i in range(pieces):
+            for i in range(1 if r == 1 else 0, pieces):
                 for m in (GATE, UP):
                     to_z(m, i, r)
 
@@ -227,28 +241,45 @@
             return carry
 
         with scope("acc#" + "#".join(f"{q}={i}" for q, i in group)):
-            lax.fori_loop(0, (span or count) // tile, step, 0)
+            if span == tile:
+                step(0, 0)
+            else:
+                lax.fori_loop(0, (span or count) // tile, step, 0)
+
+    pending = []
+
+    def enqueue(group, begin=False):
+        for t in range(count // tile):
+            pending.append(functools.partial(accumulate, group, begin=begin, start=t * tile, span=tile))
+
+    def drain():
+        while pending:
+            pending.pop(0)()
 
     def take(m, i, q, s):
-        if (q, s) == (0, 0):
-
-            @pl.when(prim)
-            def _():
-                local(m, i).wait()
-
-            @pl.when(second)
-            def _():
-                wait(slot(m, i, q, s), w_recv.at[m, number(i), number(q), s])
-
-        else:
-            with scope(f"take#m={m}#i={i}#q={q}#s={s}".replace(" ", "")):
-                wait(slot(m, i, q, s), w_recv.at[m, number(i), number(q), s])
-
-            @pl.when(prim)
-            def _():
-                if s == 0:
-                    to_y(m, i, q, slot(m, i, q, s))
-                to_core(m, i, q, s, slot(m, i, q, s))
+        for h in halves(m):
+            if (q, s) == (0, 0):
+
+                @pl.when(prim)
+                def _():
+                    local(m, i, h).wait()
+
+                @pl.when(second)
+                def _():
+                    wait(slot(m, i, q, s, h), w_recv.at[m, i, q, s, h])
+
+            else:
+                with scope(f"take#m={m}#i={i}#q={q}#s={s}#h={h}".replace(" ", "")):
+                    wait(slot(m, i, q, s, h), w_recv.at[m, number(i), number(q), s, h])
+
+                @pl.when(prim)
+                def _():
+                    if s == 0:
+                        to_y(m, i, q, h, slot(m, i, q, s, h))
+                    to_core(m, i, q, s, h, slot(m, i, q, s, h))
+
+            if pending:
+                pending.pop(0)()
 
     def take_both(i, q, rows):
         for s in rows:
@@ -265,7 +296,8 @@
     every = range(pieces)
     for i in every:
         take_both(i, 0, range(ny))
-    accumulate([(0, i) for i in every], begin=True)
+    enqueue([(0, i) for i in every], begin=True)
+    drain()
     steps = [
         ((q0, q1), (i0, i1))
         for (q0, i0), (q1, i1) in zip([(q, i) for q in late for i in every], [(q, i) for i in every for q in late])
@@ -276,81 +308,87 @@
             q, i = steps[n]
             take_both(i, q, here)
 
-    def down_to_z(place):
-        @pl.when(prim & (inside == place))
+    def down_to_z(place, core):
+        @pl.when((prim if core == 0 else second) & (inside == place))
         def _():
             for k in every:
-                for r in range(2, nz, 2):
+                for r in range(2, nz, 2) if core == 0 else [1] if place else range(3, nz, 2):
                     to_z(DOWN, k, r)
 
-        @pl.when(second & (inside == place))
-        def _():
-            for k in every:
-                for r in [1] if place else range(3, nz, 2):
-                    to_z(DOWN, k, r)
-
     for q in early:
-        for i in every:
-            take_both(i, q, here)
+        take_both(0, q, here)
     pass_on(0)
     for q in early:
-        for i in every:
-            take_both(i, q, away)
-    pass_on(1)
+        for i in every[1:]:
+            take_both(i, q, here)
+    for m in (GATE, UP):
+        for q in early:
+            for i in every if m == GATE else every[-1:]:
+                for s in away:
+                    take(m, i, q, s)
+                    if m == GATE and i < pieces - 1:
+                        take(UP, i, q, s)
+        if len(steps) > 1:
+            take(m, steps[1][1], steps[1][0], 0)
     for q in early:
-        accumulate([(q, k) for k in every])
+        enqueue([(q, i) for i in every])
     pass_on(2)
     group = []
     for n, (q, i) in enumerate(steps):
         last = n == len(steps) - 1
         if last:
-            down_to_z(0)
+            drain()
         take_both(i, q, away)
-        pass_on(n + 3)
-        if n + 4 == max(len(steps), 4):
-            down_to_z(1)
         group.append((q, i))
         if not last and (n == len(steps) - 2 or n % 2):
-            accumulate(group)
+            enqueue(group)
             group = []
+        if n == min(1, len(steps) - 1):
+            down_to_z(1, 0)
+            down_to_z(1, 1)
+        if n > 0:
+            pass_on(n + 2)
 
     def at(q, s):
         return q * ny + s
 
     parts = [flip(x, t) for t in range(1, nx)] + [x]
     subs = (other, c)
-    straight = early[:1]
+    straight = late[1:2]
 
     def sub_rows(x, k):
         return pl.ds(pl.multiple_of(x * part + k * keep, keep), keep)
 
-    def to_x(j, t):
+    def to_x(j, t, h):
         there = flip(x, t)
-        for h, k in enumerate(subs):
-            send(pb.at[j, sub_rows(there, k)], xv.at[t - 1, j, h], x_sem.at[t], x_recv.at[t, j, h], dev(z, y, there, c))
+        rows = sub_rows(there, subs[h])
+        send(pb.at[j, rows], xv.at[t - 1, j, h], x_sem.at[t], x_recv.at[t, j, h], dev(z, y, there, c))
 
     def partial(q, s, head=None):
         j = at(q, s)
         for t, p in enumerate(parts):
-            start = p * part
-            if head:
-                head(start)
-
-            def step(t, carry):
-                rows = pl.ds(pl.multiple_of(start + t * tile, tile), tile)
-                pb[j, rows, :] = jnp.dot(hid[rows, :], wd[q, s], preferred_element_type=jnp.float32).astype(jnp.bfloat16)
-                return carry
-
-            with scope(f"part#q={q}#s={s}"):
-                lax.fori_loop(0, part // tile, step, 0)
-            if q not in straight and t + 1 < nx:
-                to_x(j, t + 1)
-            if q in straight:
-
-                @pl.when(second)
-                def _():
-                    rows = pl.ds(pl.multiple_of(start, part), part)
-                    send(pb.at[j, rows], zv.at[s, rows], zv_sem, zv_recv.at[s, t], dev(near, y, x, c))
+            for h, k in enumerate(subs):
+                start = p * part + k * keep
+                if head:
+                    head(start)
+                    if (t, h) == (nx - 1, 0):
+                        down_to_z(0, 0)
+
+                def step(n, carry):
+                    rows = pl.ds(pl.multiple_of(start + n * tile, tile), tile)
+                    pb[j, rows, :] = jnp.dot(hid[rows, :], wd[q, s], preferred_element_type=jnp.float32).astype(jnp.bfloat16)
+                    return carry
+
+                with scope(f"part#q={q}#s={s}"):
+                    lax.fori_loop(0, keep // tile, step, 0)
+                if q not in straight and t + 1 < nx:
+                    to_x(j, t + 1, h)
+                if q in straight:
+
+                    @pl.when(second)
+                    def _():
+                        rows = pl.ds(pl.multiple_of(start, keep), keep)
+                        send(pb.at[j, rows], zv.at[s, rows], zv_sem, zv_recv.at[s, t, h], dev(near, y, x, c))
 
     def gather_z(q, s):
         j = at(q, s)
@@ -358,12 +396,13 @@
         @pl.when(prim)
         def _():
             for t, p in enumerate(parts):
-                rows = pl.ds(pl.multiple_of(p * part, part), part)
-                with scope(f"zwait#q={q}#s={s}"):
-                    wait(zv.at[s, rows], zv_recv.at[s, t])
-                pb[j, rows, :] = (pb[j, rows, :].astype(jnp.float32) + zv[s, rows, :].astype(jnp.float32)).astype(jnp.bfloat16)
-                if t + 1 < nx:
-                    to_x(j, t + 1)
+                for h, k in enumerate(subs):
+                    rows = sub_rows(p, k)
+                    with scope(f"zwait#q={q}#s={s}"):
+                        wait(zv.at[s, rows], zv_recv.at[s, t, h])
+                    pb[j, rows, :] = (pb[j, rows, :].astype(jnp.float32) + zv[s, rows, :].astype(jnp.float32)).astype(jnp.bfloat16)
+                    if t + 1 < nx:
+                        to_x(j, t + 1, h)
 
     def added(j, h, k):
         total = pb[j, sub_rows(x, k), :].astype(jnp.float32)
@@ -427,10 +466,8 @@
     order += [(q, 0) for q in late[1:] + early[1:]]
     order += [(q, s) for q in late + early[1:] for s in away]
     ahead = {1: [(q, 0) for q in early[:1]], ny: [(1, 0)]}
-    if early:
-        ahead[order.index((early[0], ny - 1)) + 1] = [(q, 0) for q in late[1:]]
     taken = []
-    lag, behind = 3, 5
+    lag, behind = 3, 6
     finishes, sums, adds = {}, {}, {}
     for n, (q, s) in enumerate(order):
         extra = 0
@@ -439,7 +476,7 @@
             extra = 2
         adds.setdefault(n + lag + extra, []).append((q, s))
         n = max(n, order.index((1 - q if q < 2 else q, s)))
-        finishes.setdefault(n + behind, []).append((q, s))
+        finishes.setdefault(max(n + behind, len(order) + 2), []).append((q, s))
     for n in range(len(order) + behind):
         for q, s in sums.get(n, ()):
             gather_z(q, s)
@@ -448,7 +485,8 @@
                 taken.append((q, s))
                 take_down(q, range(s, s + 1))
         if n == 0:
-            partial(*order[0], head=lambda start: accumulate(group, end=True, start=start, span=part))
+            partial(*order[0], head=lambda start: accumulate(group, end=True, start=start, span=keep))
+            down_to_z(0, 1)
         elif 0 < n < len(order):
             partial(*order[n])
         for q, s in adds.get(n, ()):
@@ -499,8 +537,8 @@
         pieces = max(rows // 128, 1)
         keep = count // n_tp
         part = count // nx
-        chunks = 8
-        tile = min(256, count)
+        chunks, cuts = 8, 2
+        tile = min(256, keep)
         bf16, f32 = jnp.bfloat16, jnp.float32
         dma = pltpu.SemaphoreType.DMA
         vmem = pl.BlockSpec(memory_space=pltpu.VMEM)
@@ -526,13 +564,13 @@
                 pltpu.VMEM((n, keep, wide), bf16),
                 pltpu.VMEM((ny, count, wide), bf16),
                 pltpu.VMEM((n, keep, wide), bf16),
-                dma((3, pieces)),
+                dma((3, pieces, cuts)),
                 dma((nx + 1,)),
                 dma((chunks, nx)),
                 dma((3, nz)),
                 dma((3, ny)),
                 dma((3,)),
-                dma((3, pieces, nz, ny)),
+                dma((3, pieces, nz, ny, cuts)),
                 dma((nx,)),
                 dma((nx, n, CORES)),
                 dma,
@@ -540,7 +578,7 @@
                 dma((CORES,)),
                 dma((n,)),
                 dma,
-                dma((ny, nx)),
+                dma((ny, nx, CORES)),
                 dma,
             ],
             compiler_params=pltpu.CompilerParams(collective_id=0, has_side_effects=True, vmem_limit_bytes=67043328),

time: 138 us -> 135 us (0.978)
  Pallas kernels: 133 us -> 131 us
    pallas_call x1, Pallas kernels: 133 us -> 131 us  [per_device(): pl.pallas_call(functools.partial(kernel, nz, ny, nx, tile), name='gated_b...]
where the time goes in v3:
time: 135 us; the launch traced here: 134 us
  Pallas kernels  131 us (97%)
  local copies, waits for them, and re-layouts  2.3 us (2%)
    pallas_call x1, Pallas kernels, per_device(): pl.pallas_call(functools.partial(kernel, nz, ny, nx, tile), name='gated_b...  131 us

profile of v3, /device:TPU:1, one launch (start us, length us, event | category | flops | bytes accessed | tf_op | source)
XLA Modules:
  0.0 133.7 jit_solution(12732037851078052444)
XLA Ops:
  0.0 131.4 %gated_block.1 = bf16[256,2048]{1,0:T(8,128)(2,1)} custom-call(bf16[1024,2048]{1,0:T(8,128)(2,1)} %tok.1, f32[1,2048]{1,0:T(1,128)} %bitcast.1, bf16[256,1408]{1,0:T(8,128)(2,1)} %gw.1, bf16[256,1408]{1,0:T(8,128)(2,1)} %uw.1, bf16[1408,256]{1,0:T(8,128)(2,1)} %dw.1), custom_call_target="tpu_custom_call" | custom-call | tf_op jit(solution)/shard_map/gated_block/pallas_call | solution.py:546
  131.4 2.3 %copy.7 = bf16[256,2048]{1,0:T(8,128)(2,1)} copy(bf16[256,2048]{1,0:T(8,128)(2,1)} %gated_block.1) | data formatting | bytes 2097152
